TPU v7x, 32 devices: a whole 2x2x4 slice. The times are simulated.
32 devices in a mesh: fs: 16 (over z, y, x), tp: 2 (over core).
Axes of the slice: x: 2, y: 2, z: 4, core: 2. Of those that a mesh axis runs over, the one named last changes fastest.
Arguments:
- gate_pre: bfloat16 [8192, 3072], P('fs', 'tp'), may hold values from -6 to 6
- up_pre: bfloat16 [8192, 3072], P('fs', 'tp'), may hold values from -6 to 6
- cotangent: bfloat16 [8192, 2048], P('fs'), may hold values from -8 to 8
- gate_weight: bfloat16 [2048, 3072], P('fs', 'tp'), may hold values from -0.125 to 0.125
- up_weight: bfloat16 [2048, 3072], P('fs', 'tp'), may hold values from -0.125 to 0.125
- down_weight: bfloat16 [2048, 3072], P('fs', 'tp'), may hold values from -0.109375 to 0.109375
Outputs:
- grad_input: bfloat16 [8192, 2048], P('fs')
- grad_down: float32 [2048, 3072], P('fs', 'tp')
All inputs are finite; a program needn't handle non-finite values.
Results may differ from a plain program's by a relative error of at most 0.014.
Values may be sent and summed in bfloat16 or wider, within the bound.
A program may use at most 128 MiB of HBM per device.

v0:
```python
import jax
import jax.numpy as jnp
from jax import lax
from jax.sharding import PartitionSpec as P


def local(gate_pre, up_pre, cotangent, gate_weight, up_weight, down_weight):
    gate = gate_pre.astype(jnp.float32)
    upper = up_pre.astype(jnp.float32)
    sigma = jax.nn.sigmoid(gate)
    hidden = (gate * sigma * upper).astype(jnp.bfloat16)
    columns = cotangent
    d_hidden = jnp.dot(
        columns,
        lax.all_gather(down_weight, "fs", axis=0, tiled=True),
        preferred_element_type=jnp.float32,
    )
    d_gate = (d_hidden * upper * sigma * (1.0 + gate * (1.0 - sigma))).astype(jnp.bfloat16)
    d_up = (d_hidden * gate * sigma).astype(jnp.bfloat16)
    pieces = lax.all_gather((gate_weight, up_weight), "fs", axis=0, tiled=True)
    first = lax.dot_general(
        d_gate, pieces[0], (((1,), (1,)), ((), ())), preferred_element_type=jnp.float32
    )
    partial_sum = first + lax.dot_general(
        d_up, pieces[1], (((1,), (1,)), ((), ())), preferred_element_type=jnp.float32
    )
    block_part = partial_sum.astype(jnp.bfloat16)
    grad_input = lax.psum(block_part, "tp").astype(jnp.float32).astype(jnp.bfloat16)
    columns = cotangent
    grad_down = lax.psum_scatter(
        lax.dot_general(
            columns, hidden, (((0,), (0,)), ((), ())), preferred_element_type=jnp.float32
        ),
        "fs",
        scatter_dimension=0,
        tiled=True,
    )
    return (grad_input, grad_down)


def solution(mesh):
    placed = (
        P("fs", "tp"),
        P("fs", "tp"),
        P("fs", None),
        P("fs", "tp"),
        P("fs", "tp"),
        P("fs", "tp"),
    )
    return jax.shard_map(
        local, mesh=mesh, in_specs=placed, out_specs=(P("fs", None), P("fs", "tp")), check_vma=False
    )
```

profile of v0, /device:TPU:9, one launch (start us, length us, event | category | flops | bytes accessed | tf_op | source)
XLA Modules:
  0.0 535.6 jit_solution(17280799704497560027)
XLA Ops:
  7.2 0.0 copy-start
  7.2 0.0 all-gather.4.cloned.1.call-start
  7.2 0.7 all-gather.4.cloned.1.call-update
  7.9 0.0 all-gather.6.cloned.1.call-start
  8.0 0.7 all-gather.6.cloned.1.call-update
  8.7 0.0 all-gather.8.cloned.1.call-start
  8.7 0.7 all-gather.8.cloned.1.call-update
  9.4 0.0 reduce-scatter.2.cloned.1.call-start
  9.4 0.0 copy-done
  9.5 8.7 %convolution_bitcast_fusion = f32[2048,1536]{0,1:T(8,128)} fusion(bf16[512,2048]{1,0:T(8,128)(2,1)S(1)} %copy-done, bf16[512,1536]{1,0:T(8,128)(2,1)} %param.7, bf16[512,1536]{1,0:T(8,128)(2,1)} %param.6), kind=kOutput, calls=%fused_computation | convolution fusion | flops 3227516928 | bytes 17825792 | tf_op jit(solution)/shard_map/dot_general | solution.py:31
  18.1 0.0 reduce-scatter.2.cloned.1.call-update
  18.2 0.0 all-reduce.2.cloned.1.call-start
  18.2 85.1 %all-gather.4.cloned.1.call-done = bf16[2048,1536]{1,0:T(8,128)(2,1)} async-done(((bf16[128,1536]{1,0:T(8,128)(2,1)}), bf16[2048,1536]{1,0:T(8,128)(2,1)}) %all-gather.4.cloned.1.call-update) | async-done | bytes 6291472 | tf_op jit(solution)/shard_map/all_gather | solution.py:15
  103.3 7.8 %fusion.20 = f32[512,1536]{1,0:T(8,128)} fusion(bf16[512,2048]{1,0:T(8,128)(2,1)S(1)} %copy-done, bf16[2048,1536]{1,0:T(8,128)(2,1)} %all-gather.4.cloned.1.call-done), kind=kOutput, calls=%fused_computation.25 | convolution fusion | flops 3221225472 | bytes 11534336 | tf_op jit(solution)/shard_map/dot_general | solution.py:13
  111.1 86.9 %all-gather.6.cloned.1.call-done = bf16[2048,1536]{1,0:T(8,128)(2,1)} async-done(((bf16[128,1536]{1,0:T(8,128)(2,1)}), bf16[2048,1536]{1,0:T(8,128)(2,1)}) %all-gather.6.cloned.1.call-update) | async-done | bytes 6291472 | tf_op jit(solution)/shard_map/all_gather | solution.py:20
  198.1 10.7 %fusion.12 = f32[512,2048]{1,0:T(8,128)} fusion(bf16[2048,1536]{1,0:T(8,128)(2,1)} %all-gather.6.cloned.1.call-done, f32[512,1536]{1,0:T(8,128)} %fusion.20, bf16[512,1536]{1,0:T(8,128)(2,1)} %param.7, bf16[512,1536]{1,0:T(8,128)(2,1)} %param.6), kind=kOutput, calls=%fused_computation.18 | convolution fusion | flops 3230662656 | bytes 16777216 | tf_op jit(solution)/shard_map/dot_general | solution.py:21
  208.7 84.1 %all-gather.8.cloned.1.call-done = bf16[2048,1536]{1,0:T(8,128)(2,1)} async-done(((bf16[128,1536]{1,0:T(8,128)(2,1)}), bf16[2048,1536]{1,0:T(8,128)(2,1)}) %all-gather.8.cloned.1.call-update) | async-done | bytes 6291472 | tf_op jit(solution)/shard_map/all_gather | solution.py:20
  292.8 10.2 %add_convert_fusion = bf16[512,2048]{1,0:T(8,128)(2,1)} fusion(f32[512,2048]{1,0:T(8,128)} %fusion.12, bf16[2048,1536]{1,0:T(8,128)(2,1)} %all-gather.8.cloned.1.call-done, f32[512,1536]{1,0:T(8,128)} %fusion.20, bf16[512,1536]{1,0:T(8,128)(2,1)} %param.6), kind=kOutput, calls=%fused_computation.5 | convolution fusion | flops 3228827648 | bytes 17301504 | tf_op jit(solution)/shard_map/dot_general | solution.py:24
  303.1 0.0 all-reduce.2.cloned.1.call-update
  303.1 198.2 %reduce-scatter.2.cloned.1.call-done = f32[128,1536]{0,1:T(8,128)} async-done(((f32[2048,1536]{0,1:T(8,128)}), f32[128,1536]{0,1:T(8,128)}) %reduce-scatter.2.cloned.1.call-update) | async-done | bytes 786448 | tf_op jit(solution)/shard_map/reduce_scatter | solution.py:30
  501.3 2.3 copy.8
  503.6 22.4 %all-reduce.2.cloned.1.call-done = bf16[512,2048]{1,0:T(8,128)(2,1)} async-done(((bf16[512,2048]{1,0:T(8,128)(2,1)}), bf16[512,2048]{1,0:T(8,128)(2,1)}) %all-reduce.2.cloned.1.call-update) | async-done | bytes 2097168 | tf_op jit(solution)/shard_map/psum | solution.py:28
  526.0 3.2 copy.10
Async XLA Ops:
  7.2 2.3 copy-start
  7.2 96.1 %all-gather.4.cloned.1.call-start = ((), (), s32[]{:S(2)}) async-start(), calls=%async_computation.1 | async-start | bytes 6684672 | tf_op jit(solution)/shard_map/all_gather | solution.py:15
  7.9 190.2 %all-gather.6.cloned.1.call-start = ((), (), s32[]{:S(2)}) async-start(), calls=%async_computation.2 | async-start | bytes 6684672 | tf_op jit(solution)/shard_map/all_gather | solution.py:20
  8.7 284.2 %all-gather.8.cloned.1.call-start = ((), (), s32[]{:S(2)}) async-start(), calls=%async_computation.3 | async-start | bytes 6684672 | tf_op jit(solution)/shard_map/all_gather | solution.py:20
  9.4 491.9 %reduce-scatter.2.cloned.1.call-start = ((), (), s32[]{:S(2)}) async-start(), calls=%async_computation.5 | async-start | bytes 13369344 | tf_op jit(solution)/shard_map/reduce_scatter | solution.py:30
  18.2 507.8 %all-reduce.2.cloned.1.call-start = ((), (), s32[]{:S(2)}) async-start(), calls=%async_computation.4 | async-start | bytes 4194304 | tf_op jit(solution)/shard_map/psum | solution.py:28
Sparse Core Ops, SparseCore 0:
  10.8 92.5 all-gather.3
  106.1 91.9 all-gather.5
  200.9 91.9 all-gather.7
  298.3 202.9 reduce-scatter.1
  504.1 21.8 all-reduce.1
where the time goes:
time: 537 us; the launch traced here: 536 us
  waiting for transfers between devices  479 us (89%)
  matrix products  37.4 us (7%)
  between operations  13.8 us (3%)
  local copies, waits for them, and re-layouts  5.45 us (1%)
    reduce_scatter x1, waiting for transfers between devices, local(): lax.psum_scatter(lax.dot_general(columns, hidden, (((0,), (0,)), ((), ())...  198 us
    all_gather x2, waiting for transfers between devices, local(): pieces = lax.all_gather((gate_weight, up_weight), 'fs', axis=0, tiled=True)  171 us
    all_gather x1, waiting for transfers between devices, local(): lax.all_gather(down_weight, 'fs', axis=0, tiled=True)  85.1 us
    psum x1, waiting for transfers between devices, local(): lax.psum(block_part, 'tp').astype(jnp.float32).astype(jnp.bfloat16)  22.4 us
  transfers between devices with their start and end apart: 5, of which 5 were waited for; matrix products, arithmetic and copies ran while one was open for 7% of the time, Pallas kernels for 0%

commit v1 on v0

v1 whole, which is shorter than its diff:
```python
import functools

import jax
import jax.numpy as jnp
from jax import lax
from jax.experimental import pallas as pl
from jax.experimental.pallas import tpu as pltpu
from jax.sharding import PartitionSpec as P

MESH = pl.DeviceIdType.MESH
F32, BF16 = jnp.float32, jnp.bfloat16
LANES = 128
VMEM_LIMIT = 60 * 1024 * 1024


def group_of(n_fs, width):
    for g in (4, 2):
        if n_fs % g == 0 and n_fs > g and width % (g * LANES) == 0:
            return g
    return 1


def place(g):
    fs, core = lax.axis_index("fs"), lax.axis_index("tp")
    base = lax.div(fs, g) * g
    return base, lax.rem(fs, g), core


def greet(g, base, me, core):
    barrier = pltpu.get_barrier_semaphore()
    for k in range(1, g):
        pl.semaphore_signal(barrier, inc=1, device_id=(base + lax.rem(me + k, g), core), device_id_type=MESH)
    pl.semaphore_signal(barrier, inc=1, device_id=(base + me, 1 - core), device_id_type=MESH)
    pl.semaphore_wait(barrier, g)


def remote(src, dst, send, recv, device):
    return pltpu.make_async_remote_copy(
        src_ref=src, dst_ref=dst, send_sem=send, recv_sem=recv, device_id=device, device_id_type=MESH
    )


def at(index, size):
    return pl.ds(pl.multiple_of(index * size, size), size)


def weights_kernel(g, *refs):
    ins, outs, (send, recv, own) = refs[:3], refs[3:6], refs[6:]
    base, me, core = place(g)
    greet(g, base, me, core)
    rows, part = ins[0].shape[0], ins[0].shape[1] // g
    copies = []
    for k in range(1, g):
        q = lax.rem(me + k, g)
        for i in (2, 0, 1):
            c = remote(ins[i].at[:, at(q, part)], outs[i].at[at(me, rows), :], send.at[i, k], recv.at[i, k], (base + q, core))
            c.start()
            copies.append(c)
    for i in range(3):
        c = pltpu.make_async_copy(ins[i].at[:, at(me, part)], outs[i].at[at(me, rows), :], own.at[i])
        c.start()
        copies.append(c)
    for c in copies:
        c.wait()


def tokens_kernel(g, gate, up, cot, gate_out, up_out, cot_out, send, recv, own):
    base, me, core = place(g)
    greet(g, base, me, core)
    rows, part = gate.shape[0], gate.shape[1] // g
    half = rows // 2
    firsts, others = [], []
    for k in range(1, g):
        q = lax.rem(me + k, g)
        c = remote(
            cot.at[at(core, half), :], cot_out.at[at(me * 2 + core, half), :], send.at[0, k], recv.at[0, k], (base + q, core)
        )
        c.start()
        firsts.append(c)
    for i, (a, b) in enumerate(((gate, gate_out), (up, up_out))):
        for k in range(1, g):
            q = lax.rem(me + k, g)
            c = remote(a.at[:, at(q, part)], b.at[at(me, rows), :], send.at[1 + i, k], recv.at[1 + i, k], (base + q, core))
            c.start()
            others.append(c)
        c = pltpu.make_async_copy(a.at[:, at(me, part)], b.at[at(me, rows), :], own.at[1 + i])
        c.start()
        others.append(c)
    c = pltpu.make_async_copy(cot, cot_out.at[at(me, rows), :], own.at[0])
    c.start()
    others.append(c)
    for k in range(1, g):
        firsts[k - 1].wait_recv()
        block = cot_out.at[at(lax.rem(me + g - k, g) * 2 + core, half), :]
        c = remote(block, block, send.at[3, k], recv.at[3, k], (base + me, 1 - core))
        c.start()
        others.append(c)
    for c in firsts:
        c.wait_send()
    for c in others:
        c.wait()


def outputs_kernel(g, part, down, out, down_out, sib, mine, got, down_got, send, recv):
    base, me, core = place(g)
    greet(g, base, me, core)
    rows, wide = out.shape
    half = wide // 2
    keep, give = at(core, half), at(1 - core, half)
    sibling = (base + me, 1 - core)
    drows, dwide = down_got.shape[1:]
    order = list(range(1, g)) + [0]
    crossed, downs, sums = {}, [], []
    for k in order:
        q = lax.rem(me + k, g)
        c = remote(part.at[at(q, rows), give], sib.at[k], send.at[0, k], recv.at[0, k], sibling)
        c.start()
        crossed[k] = c
    for k in range(1, g):
        q = lax.rem(me + k, g)
        c = remote(down.at[at(q, drows), :], down_got.at[k], send.at[1, k], recv.at[1, k], (base + q, core))
        c.start()
        downs.append(c)
    for k in order:
        q = lax.rem(me + k, g)
        crossed[k].wait_recv()
        total = part[at(q, rows), keep].astype(F32) + sib[k].astype(F32)
        mine[k] = total.astype(BF16)
        if k:
            c = remote(mine.at[k], got.at[k], send.at[2, k], recv.at[2, k], (base + q, core))
            c.start()
            sums.append(c)
    down_out[:, at(me, dwide)] = down[at(me, drows), :].astype(F32)
    for k in range(1, g):
        downs[k - 1].wait_recv()
        down_out[:, at(lax.rem(me + g - k, g), dwide)] = down_got[k].astype(F32)
    for c in sums:
        c.wait_recv()
    total = mine[0].astype(F32)
    for k in range(1, g):
        total = total + got[k].astype(F32)
    out[:, keep] = total.astype(BF16)
    last = remote(out.at[:, keep], out.at[:, keep], send.at[3, 0], recv.at[3, 0], sibling)
    last.start()
    for k in order:
        crossed[k].wait_send()
    for c in downs + sums:
        c.wait_send()
    last.wait()


def call(kernel, outs, scratch, ident, moved, *args):
    vmem = pl.BlockSpec(memory_space=pltpu.VMEM)
    return pl.pallas_call(
        kernel,
        out_shape=outs,
        in_specs=[vmem] * len(args),
        out_specs=[vmem] * len(outs),
        scratch_shapes=scratch,
        compiler_params=pltpu.CompilerParams(collective_id=ident, has_side_effects=True, vmem_limit_bytes=VMEM_LIMIT),
        cost_estimate=pl.CostEstimate(flops=0, bytes_accessed=moved * 40, transcendentals=0),
    )(*args)


def shared(g, n_fs, gate_pre, up_pre, cotangent, gate_weight, up_weight, down_weight):
    tokens, width = gate_pre.shape
    rows, depth = gate_weight.shape[0], cotangent.shape[1]
    part = width // g
    sems = pltpu.SemaphoreType.DMA
    struct = jax.ShapeDtypeStruct
    columns = [[o * g + p for o in range(n_fs // g)] for p in range(g)]
    block = struct((rows * g, part), BF16)
    blocks = call(
        functools.partial(weights_kernel, g), [block] * 3, [sems((3, g)), sems((3, g)), sems((3,))], 0,
        gate_weight.size * 6, gate_weight, up_weight, down_weight,
    )
    gather = functools.partial(lax.all_gather, axis_name="fs", axis_index_groups=columns, axis=0, tiled=True)
    down_all = gather(blocks[2])
    gate_w, up_w = gather(blocks[0]), gather(blocks[1])
    taken = struct((tokens * g, part), BF16)
    gates, ups, cots = call(
        functools.partial(tokens_kernel, g), [taken, taken, struct((tokens * g, depth), BF16)],
        [sems((4, g)), sems((4, g)), sems((3,))], 1, gate_pre.size * 8, gate_pre, up_pre, cotangent,
    )
    gate, upper = gates.astype(F32), ups.astype(F32)
    sigma = jax.nn.sigmoid(gate)
    hidden = (gate * sigma * upper).astype(BF16)
    share = lax.dot_general(cots, hidden, (((0,), (0,)), ((), ())), preferred_element_type=F32).astype(BF16)
    grad_down = lax.psum_scatter(share, "fs", scatter_dimension=0, axis_index_groups=columns, tiled=True)
    d_hidden = jnp.dot(cots, down_all, preferred_element_type=F32)
    d_gate = (d_hidden * upper * sigma * (1.0 + gate * (1.0 - sigma))).astype(BF16)
    d_up = (d_hidden * gate * sigma).astype(BF16)
    over = (((1,), (1,)), ((), ()))
    partial_sum = lax.dot_general(d_gate, gate_w, over, preferred_element_type=F32)
    partial_sum = partial_sum + lax.dot_general(d_up, up_w, over, preferred_element_type=F32)
    strip = (g, tokens, depth // 2)
    grad_input, grad_down = call(
        functools.partial(outputs_kernel, g),
        [struct((tokens, depth), BF16), struct((rows, width), F32)],
        [pltpu.VMEM(strip, BF16)] * 3 + [pltpu.VMEM((g, rows, part), BF16), sems((4, g)), sems((4, g))],
        2, cotangent.size * 8, partial_sum.astype(BF16), grad_down,
    )
    return grad_input, grad_down


def plain(gate_pre, up_pre, cotangent, gate_weight, up_weight, down_weight):
    gate = gate_pre.astype(F32)
    upper = up_pre.astype(F32)
    sigma = jax.nn.sigmoid(gate)
    hidden = (gate * sigma * upper).astype(BF16)
    share = lax.dot_general(cotangent, hidden, (((0,), (0,)), ((), ())), preferred_element_type=F32)
    grad_down = lax.psum_scatter(share, "fs", scatter_dimension=0, tiled=True)
    d_hidden = jnp.dot(cotangent, lax.all_gather(down_weight, "fs", axis=0, tiled=True), preferred_element_type=F32)
    d_gate = (d_hidden * upper * sigma * (1.0 + gate * (1.0 - sigma))).astype(BF16)
    d_up = (d_hidden * gate * sigma).astype(BF16)
    gate_w, up_w = lax.all_gather((gate_weight, up_weight), "fs", axis=0, tiled=True)
    over = (((1,), (1,)), ((), ()))
    partial_sum = lax.dot_general(d_gate, gate_w, over, preferred_element_type=F32)
    partial_sum = partial_sum + lax.dot_general(d_up, up_w, over, preferred_element_type=F32)
    grad_input = lax.psum(partial_sum.astype(BF16), "tp").astype(F32).astype(BF16)
    return grad_input, grad_down


def solution(mesh):
    n_fs, n_tp = mesh.shape["fs"], mesh.shape["tp"]

    def local(*args):
        g = group_of(n_fs, args[0].shape[1]) if n_tp == 2 else 1
        return shared(g, n_fs, *args) if g > 1 else plain(*args)

    both, rows = P("fs", "tp"), P("fs", None)
    return jax.shard_map(
        local, mesh=mesh, in_specs=(both, both, rows, both, both, both), out_specs=(rows, both), check_vma=False
    )
```

time: 537 us -> 249 us (0.46)
  waiting for transfers between devices: 479 us -> 13.8 us
  Pallas kernels: 0 us -> 169 us
  matrix products: 37.4 us -> 45.5 us
    all_gather x3, waiting for transfers between devices: 256 us -> 0.04 us  [the longest x2 0.02 us: shared(): gate_w, up_w = (gather(blocks[0]), gather(blocks[1]))]
    reduce_scatter x1, waiting for transfers between devices: 198 us -> 12.4 us  [shared(): lax.psum_scatter(share, 'fs', scatter_dimension=0, axis_index_groups=colu...]
    pallas_call x0 -> x3, Pallas kernels: none -> 169 us  [call(): pl.pallas_call(kernel, out_shape=outs, in_specs=[vmem] * len(args), out_s...]
    psum x1 -> x0, waiting for transfers between devices: 22.4 us -> none  [local(): lax.psum(block_part, 'tp').astype(jnp.float32).astype(jnp.bfloat16)]
    dot_general x4, matrix products: 37.4 us -> 45.5 us  [the longest x1 14.7 us: shared(): lax.dot_general(d_up, up_w, over, preferred_element_type=F32)]
  transfers between devices with their start and end apart: 5 -> 4, of which waited for: 5 -> 1; matrix products, arithmetic and copies ran while one was open for 7% -> 18% of each run, Pallas kernels for 0% -> 36%
where the time goes in v1:
time: 249 us; the launch traced here: 246 us
  Pallas kernels  169 us (68%)
  matrix products  45.5 us (18%)
  waiting for transfers between devices  13.8 us (6%)
  between operations  13.8 us (6%)
  local copies, waits for them, and re-layouts  4.12 us (2%)
    pallas_call x3, Pallas kernels, call(): pl.pallas_call(kernel, out_shape=outs, in_specs=[vmem] * len(args), out_s...  169 us
    dot_general x1, matrix products, shared(): lax.dot_general(d_up, up_w, over, preferred_element_type=F32)  14.7 us
    dot_general x1, matrix products, shared(): lax.dot_general(d_gate, gate_w, over, preferred_element_type=F32)  13.1 us
    reduce_scatter x1, waiting for transfers between devices, shared(): lax.psum_scatter(share, 'fs', scatter_dimension=0, axis_index_groups=colu...  12.4 us
    dot_general x1, matrix products, shared(): lax.dot_general(cots, hidden, (((0,), (0,)), ((), ())), preferred_element...  10.1 us
    dot_general x1, matrix products, shared(): d_hidden = jnp.dot(cots, down_all, preferred_element_type=F32)  7.56 us
  transfers between devices with their start and end apart: 4, of which 1 were waited for; matrix products, arithmetic and copies ran while one was open for 18% of the time, Pallas kernels for 36%

profile of v1, /device:TPU:9, one launch (start us, length us, event | category | flops | bytes accessed | tf_op | source)
XLA Modules:
  0.0 246.1 jit_solution(9976384222266677958)
XLA Ops:
  7.2 0.0 all-gather.4.cloned.1.call-start
  7.2 18.4 %shard_map.78 = (bf16[512,384]{1,0:T(8,128)(2,1)}, bf16[512,384]{1,0:T(8,128)(2,1)}, bf16[512,384]{1,0:T(8,128)(2,1)}) custom-call(bf16[128,1536]{1,0:T(8,128)(2,1)} %refs_0_.1, bf16[128,1536]{1,0:T(8,128)(2,1)} %refs_1_.1, bf16[128,1536]{1,0:T(8,128)(2,1)} %refs_2_.1), custom_call_target="tpu_custom_call" | custom-call | bytes 47185920 | tf_op jit(solution)/shard_map/pallas_call | solution.py:154
  25.6 0.0 all-gather.4.cloned.1.call-update
  25.6 0.0 all-gather.6.cloned.1.call-start
  25.7 0.7 all-gather.6.cloned.1.call-update
  26.4 0.0 all-gather.8.cloned.1.call-start
  26.4 0.7 all-gather.8.cloned.1.call-update
  27.1 0.0 reduce-scatter.2.cloned.1.call-start
  27.2 88.9 %shard_map.77 = (bf16[2048,384]{1,0:T(8,128)(2,1)}, bf16[2048,384]{1,0:T(8,128)(2,1)}, bf16[2048,2048]{1,0:T(8,128)(2,1)}) custom-call(bf16[512,1536]{1,0:T(8,128)(2,1)} %gate.1, bf16[512,1536]{1,0:T(8,128)(2,1)} %up.1, bf16[512,2048]{1,0:T(8,128)(2,1)} %cot.1), custom_call_target="tpu_custom_call" | custom-call | bytes 251658240 | tf_op jit(solution)/shard_map/pallas_call | solution.py:154
  116.1 10.1 %convolution_convert_fusion = bf16[2048,384]{1,0:T(8,128)(2,1)} fusion(bf16[2048,2048]{1,0:T(8,128)(2,1)} %get-tuple-element.8, bf16[2048,384]{1,0:T(8,128)(2,1)} %get-tuple-element.10, bf16[2048,384]{1,0:T(8,128)(2,1)} %get-tuple-element.11), kind=kOutput, calls=%fused_computation.17 | convolution fusion | flops 3228303360 | bytes 13107200 | tf_op jit(solution)/shard_map/dot_general | solution.py:188
  126.2 0.0 reduce-scatter.2.cloned.1.call-update
  126.2 0.0 all-gather.4.cloned.1.call-done
  126.3 7.6 %fusion.20 = f32[2048,384]{1,0:T(8,128)S(1)} fusion(bf16[2048,2048]{1,0:T(8,128)(2,1)} %get-tuple-element.8, bf16[2048,384]{1,0:T(8,128)(2,1)} %all-gather.4.cloned.1.call-done), kind=kOutput, calls=%fused_computation.25 | convolution fusion | flops 3221225472 | bytes 13107200 | tf_op jit(solution)/shard_map/dot_general | solution.py:190
  133.8 0.0 all-gather.6.cloned.1.call-done
  133.9 13.1 %fusion.12 = f32[2048,2048]{1,0:T(8,128)} fusion(bf16[2048,384]{1,0:T(8,128)(2,1)} %all-gather.6.cloned.1.call-done, f32[2048,384]{1,0:T(8,128)S(1)} %fusion.20, bf16[2048,384]{1,0:T(8,128)(2,1)} %get-tuple-element.10, bf16[2048,384]{1,0:T(8,128)(2,1)} %get-tuple-element.11), kind=kOutput, calls=%fused_computation.18 | convolution fusion | flops 3230662656 | bytes 24641536 | tf_op jit(solution)/shard_map/dot_general | solution.py:194
  146.9 0.0 all-gather.8.cloned.1.call-done
  146.9 14.7 %add_convert_fusion.part = bf16[2048,2048]{1,0:T(8,128)(2,1)} fusion(f32[2048,2048]{1,0:T(8,128)} %fusion.12, bf16[2048,384]{1,0:T(8,128)(2,1)} %all-gather.8.cloned.1.call-done, f32[2048,384]{1,0:T(8,128)S(1)} %fusion.20, bf16[2048,384]{1,0:T(8,128)(2,1)} %get-tuple-element.11), kind=kOutput, calls=%fused_computation | convolution fusion | flops 3235119104 | bytes 31457280 | tf_op jit(solution)/shard_map/dot_general | solution.py:195
  161.7 12.4 %reduce-scatter.2.cloned.1.call-done.down = bf16[512,384]{1,0:T(8,128)(2,1)} async-done(((bf16[2048,384]{1,0:T(8,128)(2,1)}), bf16[512,384]{1,0:T(8,128)(2,1)}) %reduce-scatter.2.cloned.1.call-update) | async-done | bytes 393232 | tf_op jit(solution)/shard_map/reduce_scatter | solution.py:189
  174.0 61.5 %shard_map.79 = (bf16[512,2048]{1,0:T(8,128)(2,1)}, f32[128,1536]{1,0:T(8,128)}) custom-call(bf16[2048,2048]{1,0:T(8,128)(2,1)} %add_convert_fusion.part, bf16[512,384]{1,0:T(8,128)(2,1)} %reduce-scatter.2.cloned.1.call-done.down), custom_call_target="tpu_custom_call" | custom-call | bytes 335544320 | tf_op jit(solution)/shard_map/pallas_call | solution.py:154
  235.5 0.0 copy-start
  235.5 3.2 %copy.10 = bf16[512,2048]{1,0:T(8,128)(2,1)} copy(bf16[512,2048]{1,0:T(8,128)(2,1)} %get-tuple-element.16) | data formatting | bytes 4194304
  238.7 0.0 copy-done
  238.7 0.9 copy.11
Async XLA Ops:
  7.2 119.1 %all-gather.4.cloned.1.call-start = ((), (), s32[]{:S(2)}) async-start(), calls=%async_computation.1 | async-start | bytes 1966080 | tf_op jit(solution)/shard_map/all_gather | solution.py:178
  25.6 108.2 %all-gather.6.cloned.1.call-start = ((), (), s32[]{:S(2)}) async-start(), calls=%async_computation.2 | async-start | bytes 1966080 | tf_op jit(solution)/shard_map/all_gather | solution.py:179
  26.4 120.5 %all-gather.8.cloned.1.call-start = ((), (), s32[]{:S(2)}) async-start(), calls=%async_computation.3 | async-start | bytes 1966080 | tf_op jit(solution)/shard_map/all_gather | solution.py:179
  27.1 146.9 %reduce-scatter.2.cloned.1.call-start = ((), (), s32[]{:S(2)}) async-start(), calls=%async_computation.4 | async-start | bytes 1966080 | tf_op jit(solution)/shard_map/reduce_scatter | solution.py:189
  235.5 3.2 %copy-start = (f32[128,1536]{1,0:T(8,128)S(1)}, f32[128,1536]{1,0:T(8,128)}, u32[]{:S(2)}) copy-start(f32[128,1536]{1,0:T(8,128)} %get-tuple-element.17) | copy-start | bytes 2359300
Sparse Core Ops, SparseCore 0:
  25.8 36.8 all-gather.3
  64.3 35.8 all-gather.5
  101.8 35.8 all-gather.7
  140.4 33.5 reduce-scatter.1

commit v2 on v1

v2 whole, which is shorter than its diff:
```python
import functools

import jax
import jax.numpy as jnp
from jax import lax
from jax.experimental import pallas as pl
from jax.experimental.pallas import tpu as pltpu
from jax.sharding import PartitionSpec as P

MESH = pl.DeviceIdType.MESH
F32, BF16 = jnp.float32, jnp.bfloat16
LANES = 128
VMEM_LIMIT = 60 * 1024 * 1024


def group_of(n_fs, width):
    return 4 if n_fs % 4 == 0 and n_fs > 4 and width % (4 * LANES) == 0 else 1


def place(g):
    fs, core = lax.axis_index("fs"), lax.axis_index("tp")
    return lax.div(fs, g) * g, lax.rem(fs, g), core


def greet(devices):
    barrier = pltpu.get_barrier_semaphore()
    for device in devices:
        pl.semaphore_signal(barrier, inc=1, device_id=device, device_id_type=MESH)
    pl.semaphore_wait(barrier, len(devices))


def remote(src, dst, send, recv, device):
    return pltpu.make_async_remote_copy(
        src_ref=src, dst_ref=dst, send_sem=send, recv_sem=recv, device_id=device, device_id_type=MESH
    )


def at(index, size):
    return pl.ds(pl.multiple_of(index * size, size), size)


def peers(g, base, me, core):
    return [(base + lax.rem(me + k, g), core) for k in range(1, g)]


def square(base, me, core):
    x, y = lax.rem(me, 2), lax.div(me, 2)
    xn, yn = y * 2 + (1 - x), (1 - y) * 2 + x
    return xn, yn, 3 - me, (base + xn, core), (base + yn, core), (base + me, 1 - core)


def swap_kernel(g, n, *refs):
    ins, outs, (send, recv, own) = refs[:n], refs[n : 2 * n], refs[2 * n :]
    base, me, core = place(g)
    greet(peers(g, base, me, core))
    rows, part = ins[0].shape[0], ins[0].shape[1] // g
    copies = []
    for k in range(1, g):
        q = lax.rem(me + k, g)
        for i in range(n):
            c = remote(ins[i].at[:, at(q, part)], outs[i].at[at(me, rows), :], send.at[i, k], recv.at[i, k], (base + q, core))
            c.start()
            copies.append(c)
    for i in range(n):
        c = pltpu.make_async_copy(ins[i].at[:, at(me, part)], outs[i].at[at(me, rows), :], own.at[i])
        c.start()
        copies.append(c)
    for c in copies:
        c.wait()


def tokens_kernel(g, n_out, cot, block, cot_out, gathered, send, recv, zsend, zrecv, own):
    base, me, core = place(g)
    outer = lax.div(base, g)
    xn, yn, far, xdev, ydev, sibling = square(base, me, core)
    others = [(lax.rem(outer + j, n_out) * g + me, core) for j in range(1, n_out)]
    greet([xdev, ydev, sibling] + others)
    half, wide = cot.shape[0] // 2, cot.shape[1] // 2
    cols = [pl.ds(0, wide), pl.ds(wide, wide)]
    mine = at(core, half)
    piece = lambda owner, i: cot_out.at[at(owner * 2 + core, half), cols[i]]
    started, passed = [], []

    def go(n, a, b, device):
        c = remote(a, b, send.at[n], recv.at[n], device)
        c.start()
        started.append(c)
        return c

    def pass_on(n, owner, i):
        c = remote(piece(owner, i), piece(owner, i), send.at[n], recv.at[n], sibling)
        c.start()
        passed.append(c)

    x0 = go(0, cot.at[mine, cols[0]], piece(me, 0), xdev)
    y1 = go(1, cot.at[mine, cols[1]], piece(me, 1), ydev)
    x1 = go(2, cot.at[mine, cols[1]], piece(me, 1), xdev)
    y0 = go(3, cot.at[mine, cols[0]], piece(me, 0), ydev)
    rows = block.shape[0]
    for j in range(1, n_out):
        c = remote(block, gathered.at[at(outer, rows), :], zsend.at[j], zrecv.at[j], others[j - 1])
        c.start()
        passed.append(c)
    for i, (a, b) in enumerate(((cot, cot_out.at[at(me, 2 * half), :]), (block, gathered.at[at(outer, rows), :]))):
        c = pltpu.make_async_copy(a, b, own.at[i])
        c.start()
        passed.append(c)
    x0.wait_recv()
    fy = go(4, piece(xn, 0), piece(xn, 0), ydev)
    pass_on(6, xn, 0)
    y1.wait_recv()
    fx = go(5, piece(yn, 1), piece(yn, 1), xdev)
    pass_on(7, yn, 1)
    x1.wait_recv()
    pass_on(8, xn, 1)
    y0.wait_recv()
    pass_on(9, yn, 0)
    fy.wait_recv()
    pass_on(10, far, 0)
    fx.wait_recv()
    pass_on(11, far, 1)
    for c in started:
        c.wait_send()
    for c in passed:
        c.wait()


def middle_kernel(g, gate, up, cots, down, hidden, d_gate, d_up, gates, ups, dh, send, recv, own):
    base, me, core = place(g)
    greet(peers(g, base, me, core))
    rows, part = gate.shape[0], gate.shape[1] // g
    copies = {}
    for k in range(1, g):
        q = lax.rem(me + k, g)
        for i, (a, b) in enumerate(((gate, gates), (up, ups))):
            c = remote(a.at[:, at(q, part)], b.at[at(me, rows), :], send.at[i, k], recv.at[i, k], (base + q, core))
            c.start()
            copies[i, k] = c
    for i, (a, b) in enumerate(((gate, gates), (up, ups))):
        c = pltpu.make_async_copy(a.at[:, at(me, part)], b.at[at(me, rows), :], own.at[i])
        c.start()
        copies[i, 0] = c
    tile = rows // 2

    def multiply(i, carry):
        dh[at(i, tile), :] = jnp.dot(cots[at(i, tile), :], down[...], preferred_element_type=F32)
        return carry

    lax.fori_loop(0, 2 * g, multiply, 0)
    strip = rows // 16
    for k in range(g):
        for i in range(2):
            if k:
                copies[i, k].wait_recv()
            else:
                copies[i, k].wait()
        owner = lax.rem(me + g - k, g)

        def pointwise(i, carry):
            r = at(owner * 16 + i, strip)
            gv, uv, dv = gates[r, :].astype(F32), ups[r, :].astype(F32), dh[r, :]
            s = jax.nn.sigmoid(gv)
            gs = gv * s
            hidden[r, :] = (gs * uv).astype(BF16)
            d_gate[r, :] = (dv * uv * s * (1.0 + gv * (1.0 - s))).astype(BF16)
            d_up[r, :] = (dv * gs).astype(BF16)
            return carry

        lax.fori_loop(0, 16, pointwise, 0)
    for k in range(1, g):
        for i in range(2):
            copies[i, k].wait_send()


OVER = (((1,), (1,)), ((), ()))


def input_kernel(g, d_gate, d_up, gate_w, up_w, out, give_buf, sib, mine, got, halves, send, recv):
    base, me, core = place(g)
    xn, yn, far, xdev, ydev, sibling = square(base, me, core)
    greet([xdev, ydev, sibling])
    rows, wide = out.shape[0], out.shape[1] // 2
    keep = at(core, wide)
    tile = rows // 2
    top, low = pl.ds(0, tile), pl.ds(tile, tile)
    sends, waits = [], []

    def product(side, owner, dst):
        cols = at(side, wide)

        def step(i, carry):
            r = at(owner * 2 + i, tile)
            total = lax.dot_general(d_gate[r, :], gate_w[cols, :], OVER, preferred_element_type=F32)
            total = total + lax.dot_general(d_up[r, :], up_w[cols, :], OVER, preferred_element_type=F32)
            dst[at(i, tile), :] = total.astype(BF16)
            return carry

        lax.fori_loop(0, 2, step, 0)

    def add(dst, where, src):
        dst[where, :] = (dst[where, :].astype(F32) + src[...].astype(F32)).astype(BF16)

    def go(n, a, b, device):
        c = remote(a, b, send.at[n], recv.at[n], device)
        c.start()
        sends.append(c)
        return c

    def chunk(k, owner):
        product(1 - core, owner, give_buf.at[k])
        c = go(k, give_buf.at[k], sib.at[k], sibling)
        product(core, owner, mine.at[k])
        c.wait_recv()
        add(mine.at[k], pl.ds(0, rows), sib.at[k])

    chunk(0, far)
    hx = go(4, mine.at[0, top, :], halves.at[0], xdev)
    hy = go(5, mine.at[0, low, :], halves.at[1], ydev)
    chunk(1, xn)
    waits.append(go(6, mine.at[1, top, :], got.at[0, top, :], xdev))
    chunk(2, yn)
    waits.append(go(7, mine.at[2, low, :], got.at[1, low, :], ydev))
    hy.wait_recv()
    add(mine.at[1], low, halves.at[1])
    waits.append(go(8, mine.at[1, low, :], got.at[0, low, :], xdev))
    hx.wait_recv()
    add(mine.at[2], top, halves.at[0])
    waits.append(go(9, mine.at[2, top, :], got.at[1, top, :], ydev))
    chunk(3, me)
    lasts = []
    for n, where, ready in ((10, top, (0, 3)), (11, low, (1, 2))):
        for i in ready:
            waits[i].wait_recv()
        total = mine[3, where, :].astype(F32) + got[0, where, :].astype(F32) + got[1, where, :].astype(F32)
        out[where, keep] = total.astype(BF16)
        lasts.append(go(n, out.at[where, keep], out.at[where, keep], sibling))
    for c in lasts:
        c.wait_recv()
    for c in sends:
        c.wait_send()


def down_kernel(g, down, out, got, send, recv):
    base, me, core = place(g)
    greet(peers(g, base, me, core))
    rows, wide = got.shape[1:]
    copies = []
    for k in range(1, g):
        q = lax.rem(me + k, g)
        c = remote(down.at[at(q, rows), :], got.at[k], send.at[k], recv.at[k], (base + q, core))
        c.start()
        copies.append(c)
    out[:, at(me, wide)] = down[at(me, rows), :].astype(F32)
    for k in range(1, g):
        copies[k - 1].wait_recv()
        out[:, at(lax.rem(me + g - k, g), wide)] = got[k].astype(F32)
    for c in copies:
        c.wait_send()


def call(kernel, outs, scratch, ident, cost, *args):
    vmem = pl.BlockSpec(memory_space=pltpu.VMEM)
    return pl.pallas_call(
        kernel,
        out_shape=outs,
        in_specs=[vmem] * len(args),
        out_specs=[vmem] * len(outs),
        scratch_shapes=scratch,
        compiler_params=pltpu.CompilerParams(collective_id=ident, has_side_effects=True, vmem_limit_bytes=VMEM_LIMIT),
        cost_estimate=pl.CostEstimate(flops=0, bytes_accessed=cost, transcendentals=0),
    )(*args)


def shared(g, n_fs, gate_pre, up_pre, cotangent, gate_weight, up_weight, down_weight):
    tokens, width = gate_pre.shape
    rows, depth = gate_weight.shape[0], cotangent.shape[1]
    part, n_out, all_tokens = width // g, n_fs // g, tokens * g
    sems, vmem = pltpu.SemaphoreType.DMA, pltpu.VMEM
    struct = jax.ShapeDtypeStruct
    us = 3_000_000
    columns = [[o * g + p for o in range(n_out)] for p in range(g)]
    gather = functools.partial(lax.all_gather, axis_name="fs", axis_index_groups=columns, axis=0, tiled=True)

    def swap(ident, *weights):
        n = len(weights)
        return call(
            functools.partial(swap_kernel, g, n), [struct((rows * g, part), BF16)] * n,
            [sems((n, g)), sems((n, g)), sems((n,))], ident, 7 * n * us, *weights,
        )

    down_all = gather(swap(0, down_weight)[0])
    gate_block, up_block = swap(1, gate_weight, up_weight)
    up_w = gather(up_block)
    cots, gate_w = call(
        functools.partial(tokens_kernel, g, n_out), [struct((all_tokens, depth), BF16), struct((depth, part), BF16)],
        [sems((12,)), sems((12,)), sems((n_out,)), sems((n_out,)), sems((2,))], 2, 40 * us, cotangent, gate_block,
    )
    wide = struct((all_tokens, part), BF16)
    hidden, d_gate, d_up = call(
        functools.partial(middle_kernel, g), [wide] * 3,
        [vmem(wide.shape, BF16)] * 2 + [vmem(wide.shape, F32), sems((2, g)), sems((2, g)), sems((2,))],
        3, 40 * us, gate_pre, up_pre, cots, down_all,
    )
    share = lax.dot_general(cots, hidden, (((0,), (0,)), ((), ())), preferred_element_type=F32).astype(BF16)
    grad_block = lax.psum_scatter(share, "fs", scatter_dimension=0, axis_index_groups=columns, tiled=True)
    side = depth // 2
    grad_input = call(
        functools.partial(input_kernel, g), [struct((tokens, depth), BF16)],
        [vmem((4, tokens, side), BF16)] * 3 + [vmem((2, tokens, side), BF16), vmem((2, tokens // 2, side), BF16)]
        + [sems((12,)), sems((12,))],
        4, 50 * us, d_gate, d_up, gate_w, up_w,
    )[0]
    grad_down = call(
        functools.partial(down_kernel, g), [struct((rows, width), F32)],
        [vmem((g, rows, part), BF16), sems((g,)), sems((g,))], 5, 6 * us, grad_block,
    )[0]
    return grad_input, grad_down


def plain(gate_pre, up_pre, cotangent, gate_weight, up_weight, down_weight):
    gate = gate_pre.astype(F32)
    upper = up_pre.astype(F32)
    sigma = jax.nn.sigmoid(gate)
    hidden = (gate * sigma * upper).astype(BF16)
    share = lax.dot_general(cotangent, hidden, (((0,), (0,)), ((), ())), preferred_element_type=F32)
    grad_down = lax.psum_scatter(share, "fs", scatter_dimension=0, tiled=True)
    d_hidden = jnp.dot(cotangent, lax.all_gather(down_weight, "fs", axis=0, tiled=True), preferred_element_type=F32)
    d_gate = (d_hidden * upper * sigma * (1.0 + gate * (1.0 - sigma))).astype(BF16)
    d_up = (d_hidden * gate * sigma).astype(BF16)
    gate_w, up_w = lax.all_gather((gate_weight, up_weight), "fs", axis=0, tiled=True)
    over = (((1,), (1,)), ((), ()))
    partial_sum = lax.dot_general(d_gate, gate_w, over, preferred_element_type=F32)
    partial_sum = partial_sum + lax.dot_general(d_up, up_w, over, preferred_element_type=F32)
    grad_input = lax.psum(partial_sum.astype(BF16), "tp").astype(F32).astype(BF16)
    return grad_input, grad_down


def solution(mesh):
    n_fs, n_tp = mesh.shape["fs"], mesh.shape["tp"]

    def local(*args):
        g = group_of(n_fs, args[0].shape[1]) if n_tp == 2 else 1
        return shared(g, n_fs, *args) if g > 1 else plain(*args)

    both, rows = P("fs", "tp"), P("fs", None)
    return jax.shard_map(
        local, mesh=mesh, in_specs=(both, both, rows, both, both, both), out_specs=(rows, both), check_vma=False
    )
```

time: 249 us -> 215 us (0.86); the launches traced: 246 us -> 215 us
  matrix products: 45.5 us -> 9.5 us
  Pallas kernels: 169 us -> 187 us
  waiting for transfers between devices: 13.8 us -> 0.11 us
    dot_general x3 -> x0, matrix products: 35.4 us -> none  [the longest x1 14.7 us: shared(): lax.dot_general(d_up, up_w, over, preferred_element_type=F32)]
    pallas_call x3 -> x6, Pallas kernels: 169 us -> 187 us  [call(): pl.pallas_call(kernel, out_shape=outs, in_specs=[vmem] * len(args), out_s...]
    reduce_scatter x1, waiting for transfers between devices: 12.4 us -> 0.02 us  [shared(): lax.psum_scatter(share, 'fs', scatter_dimension=0, axis_index_groups=colu...]
  transfers between devices with their start and end apart: 4 -> 3, of which waited for: 1 -> 0; matrix products, arithmetic and copies ran while one was open for 18% -> 4% of each run, Pallas kernels for 36% -> 78%
where the time goes in v2:
time: 215 us
  Pallas kernels  187 us (87%)
  between operations  13.8 us (6%)
  matrix products  9.5 us (4%)
  local copies, waits for them, and re-layouts  4.12 us (2%)
    pallas_call x6, Pallas kernels, call(): pl.pallas_call(kernel, out_shape=outs, in_specs=[vmem] * len(args), out_s...  187 us
    dot_general x1, matrix products, shared(): lax.dot_general(cots, hidden, (((0,), (0,)), ((), ())), preferred_element...  9.5 us
  transfers between devices with their start and end apart: 3, of which 0 were waited for; matrix products, arithmetic and copies ran while one was open for 4% of the time, Pallas kernels for 78%

profile of v2, /device:TPU:9, one launch (start us, length us, event | category | flops | bytes accessed | tf_op | source)
XLA Modules:
  0.0 215.0 jit_solution(11089738426133326443)
XLA Ops:
  7.2 0.0 all-gather.3.cloned.1.call-start
  7.2 9.6 %shard_map.79 = bf16[512,384]{1,0:T(8,128)(2,1)} custom-call(bf16[128,1536]{1,0:T(8,128)(2,1)} %refs_0_.3), custom_call_target="tpu_custom_call" | custom-call | bytes 21000000 | tf_op jit(solution)/shard_map/pallas_call | solution.py:263
  16.9 0.0 all-gather.3.cloned.1.call-update
  16.9 0.0 all-gather.5.cloned.1.call-start
  16.9 13.4 %shard_map.77 = (bf16[512,384]{1,0:T(8,128)(2,1)}, bf16[512,384]{1,0:T(8,128)(2,1)}) custom-call(bf16[128,1536]{1,0:T(8,128)(2,1)} %refs_0_.2, bf16[128,1536]{1,0:T(8,128)(2,1)} %refs_1_.1), custom_call_target="tpu_custom_call" | custom-call | bytes 42000000 | tf_op jit(solution)/shard_map/pallas_call | solution.py:263
  30.4 0.0 all-gather.5.cloned.1.call-update
  30.4 0.0 reduce-scatter.2.cloned.1.call-start
  30.5 61.3 %shard_map.78 = (bf16[2048,2048]{1,0:T(8,128)(2,1)}, bf16[2048,384]{1,0:T(8,128)(2,1)}) custom-call(bf16[512,2048]{1,0:T(8,128)(2,1)} %cot.1, bf16[512,384]{1,0:T(8,128)(2,1)} %get-tuple-element.9.block), custom_call_target="tpu_custom_call" | custom-call | bytes 120000000 | tf_op jit(solution)/shard_map/pallas_call | solution.py:263
  91.7 0.0 all-gather.3.cloned.1.call-done.down
  91.8 45.3 %shard_map.80 = (bf16[2048,384]{1,0:T(8,128)(2,1)}, bf16[2048,384]{1,0:T(8,128)(2,1)}, bf16[2048,384]{1,0:T(8,128)(2,1)}) custom-call(bf16[512,1536]{1,0:T(8,128)(2,1)} %gate.1, bf16[512,1536]{1,0:T(8,128)(2,1)} %up.1, bf16[2048,2048]{1,0:T(8,128)(2,1)} %get-tuple-element.10.cots, bf16[2048,384]{1,0:T(8,128)(2,1)} %all-gather.3.cloned.1.call-done.down), custom_call_target="tpu_custom_call" | custom-call | bytes 120000000 | tf_op jit(solution)/shard_map/pallas_call | solution.py:263
  137.0 9.5 %convolution_convert_fusion = bf16[2048,384]{1,0:T(8,128)(2,1)} fusion(bf16[2048,2048]{1,0:T(8,128)(2,1)} %get-tuple-element.10.cots, bf16[2048,384]{1,0:T(8,128)(2,1)} %get-tuple-element.15), kind=kOutput, calls=%fused_computation | convolution fusion | flops 3222011904 | bytes 11534336 | tf_op jit(solution)/shard_map/dot_general | solution.py:304
  146.5 0.0 reduce-scatter.2.cloned.1.call-update
  146.6 0.0 all-gather.5.cloned.1.call-done.up_w
  146.6 48.0 %shard_map.81 = bf16[512,2048]{1,0:T(8,128)(2,1)} custom-call(bf16[2048,384]{1,0:T(8,128)(2,1)} %get-tuple-element.11.d_gate, bf16[2048,384]{1,0:T(8,128)(2,1)} %get-tuple-element.12.d_up, bf16[2048,384]{1,0:T(8,128)(2,1)} %get-tuple-element.13.gate_w, bf16[2048,384]{1,0:T(8,128)(2,1)} %all-gather.5.cloned.1.call-done.up_w), custom_call_target="tpu_custom_call" | custom-call | bytes 150000000 | tf_op jit(solution)/shard_map/pallas_call | solution.py:263
  194.7 0.0 reduce-scatter.2.cloned.1.call-done.down
  194.7 9.6 %shard_map.82 = f32[128,1536]{1,0:T(8,128)} custom-call(bf16[512,384]{1,0:T(8,128)(2,1)} %reduce-scatter.2.cloned.1.call-done.down), custom_call_target="tpu_custom_call" | custom-call | bytes 18000000 | tf_op jit(solution)/shard_map/pallas_call | solution.py:263
  204.3 0.0 copy-start
  204.3 3.2 %copy.10 = bf16[512,2048]{1,0:T(8,128)(2,1)} copy(bf16[512,2048]{1,0:T(8,128)(2,1)} %shard_map.81) | data formatting | bytes 4194304
  207.6 0.0 copy-done
  207.6 0.9 copy.11
Async XLA Ops:
  7.2 84.6 %all-gather.3.cloned.1.call-start = ((), (), s32[]{:S(2)}) async-start(), calls=%async_computation.1 | async-start | bytes 1966080 | tf_op jit(solution)/shard_map/all_gather | solution.py:291
  16.9 129.7 %all-gather.5.cloned.1.call-start = ((), (), s32[]{:S(2)}) async-start(), calls=%async_computation.2 | async-start | bytes 1966080 | tf_op jit(solution)/shard_map/all_gather | solution.py:293
  30.4 164.3 %reduce-scatter.2.cloned.1.call-start = ((), (), s32[]{:S(2)}) async-start(), calls=%async_computation.3 | async-start | bytes 1966080 | tf_op jit(solution)/shard_map/reduce_scatter | solution.py:305
  204.3 3.2 %copy-start = (f32[128,1536]{1,0:T(8,128)S(1)}, f32[128,1536]{1,0:T(8,128)}, u32[]{:S(2)}) copy-start(f32[128,1536]{1,0:T(8,128)} %shard_map.82) | copy-start | bytes 2359300
Sparse Core Ops, SparseCore 0:
  17.0 55.2 all-gather.2
  73.9 42.8 all-gather.4
  146.7 31.9 reduce-scatter.1

commit v3 on v2

--- a/solution.py
+++ b/solution.py
@@ -49,37 +49,46 @@
     return xn, yn, 3 - me, (base + xn, core), (base + yn, core), (base + me, 1 - core)
 
 
-def swap_kernel(g, n, *refs):
-    ins, outs, (send, recv, own) = refs[:n], refs[n : 2 * n], refs[2 * n :]
-    base, me, core = place(g)
-    greet(peers(g, base, me, core))
-    rows, part = ins[0].shape[0], ins[0].shape[1] // g
-    copies = []
-    for k in range(1, g):
-        q = lax.rem(me + k, g)
-        for i in range(n):
-            c = remote(ins[i].at[:, at(q, part)], outs[i].at[at(me, rows), :], send.at[i, k], recv.at[i, k], (base + q, core))
+class Ring:
+    def __init__(self, array, rows, outer, n_out, base, me, core, g, send, recv, line):
+        self.array, self.half, self.outer, self.n = array, rows // 2, outer, n_out
+        self.send, self.recv, self.line, self.copies = send, recv, line, []
+        self.devices = [(lax.rem(outer + d, n_out) * g + me, core) for d in (1, n_out - 1)]
+
+    def step(self, s):
+        if s:
+            for c in self.copies[-2:]:
+                c.wait_recv()
+        if s == self.n - 1:
+            return
+        for way in range(2):
+            owner = lax.rem(self.outer + (self.n - s if way == 0 else s), self.n)
+            block = self.array.at[at(owner * 2 + way, self.half), :]
+            n = s * 2 + way
+            c = remote(block, block, self.send.at[self.line, n], self.recv.at[self.line, n], self.devices[way])
             c.start()
-            copies.append(c)
-    for i in range(n):
-        c = pltpu.make_async_copy(ins[i].at[:, at(me, part)], outs[i].at[at(me, rows), :], own.at[i])
-        c.start()
-        copies.append(c)
-    for c in copies:
-        c.wait()
-
-
-def tokens_kernel(g, n_out, cot, block, cot_out, gathered, send, recv, zsend, zrecv, own):
+            self.copies.append(c)
+
+    def finish(self):
+        for c in self.copies:
+            c.wait_send()
+
+
+def ring_devices(outer, n_out, me, core, g):
+    return [(lax.rem(outer + d, n_out) * g + me, core) for d in (1, n_out - 1)]
+
+
+def tokens_kernel(g, n_out, cot, down, gate, up, cot_out, down_all, gate_all, up_block, send, recv, wsend, wrecv, zsend, zrecv, own):
     base, me, core = place(g)
     outer = lax.div(base, g)
     xn, yn, far, xdev, ydev, sibling = square(base, me, core)
-    others = [(lax.rem(outer + j, n_out) * g + me, core) for j in range(1, n_out)]
-    greet([xdev, ydev, sibling] + others)
+    greet(peers(g, base, me, core) + [sibling] + ring_devices(outer, n_out, me, core, g))
     half, wide = cot.shape[0] // 2, cot.shape[1] // 2
+    rows, part = down.shape[0], down.shape[1] // g
     cols = [pl.ds(0, wide), pl.ds(wide, wide)]
     mine = at(core, half)
     piece = lambda owner, i: cot_out.at[at(owner * 2 + core, half), cols[i]]
-    started, passed = [], []
+    started, passed, swaps = [], [], {}
 
     def go(n, a, b, device):
         c = remote(a, b, send.at[n], recv.at[n], device)
@@ -92,42 +101,81 @@
         c.start()
         passed.append(c)
 
+    def local_copy(i, a, b):
+        c = pltpu.make_async_copy(a, b, own.at[i])
+        c.start()
+        return c
+
+    def swap(i, a, b):
+        swaps[i] = []
+        for k in range(1, g):
+            q = lax.rem(me + k, g)
+            c = remote(a.at[:, at(q, part)], b, wsend.at[i, k], wrecv.at[i, k], (base + q, core))
+            c.start()
+            swaps[i].append(c)
+        return local_copy(i, a.at[:, at(me, part)], b)
+
+    place_of = at(outer * g + me, rows)
+    own_down = swap(0, down, down_all.at[place_of, :])
+    own_gate = swap(1, gate, gate_all.at[place_of, :])
     x0 = go(0, cot.at[mine, cols[0]], piece(me, 0), xdev)
     y1 = go(1, cot.at[mine, cols[1]], piece(me, 1), ydev)
     x1 = go(2, cot.at[mine, cols[1]], piece(me, 1), xdev)
     y0 = go(3, cot.at[mine, cols[0]], piece(me, 0), ydev)
-    rows = block.shape[0]
-    for j in range(1, n_out):
-        c = remote(block, gathered.at[at(outer, rows), :], zsend.at[j], zrecv.at[j], others[j - 1])
-        c.start()
-        passed.append(c)
-    for i, (a, b) in enumerate(((cot, cot_out.at[at(me, 2 * half), :]), (block, gathered.at[at(outer, rows), :]))):
-        c = pltpu.make_async_copy(a, b, own.at[i])
-        c.start()
-        passed.append(c)
+    own_cot = local_copy(3, cot, cot_out.at[at(me, 2 * half), :])
+    rings = []
+    for i, array, mine_copy in ((0, down_all, own_down), (1, gate_all, own_gate)):
+        mine_copy.wait()
+        for c in swaps[i]:
+            c.wait_recv()
+        rings.append(Ring(array, rows * g, outer, n_out, base, me, core, g, zsend, zrecv, i))
+        rings[i].step(0)
+    steps = [(i, n) for n in range(1, n_out) for i in range(2)]
+
+    def turn():
+        if steps:
+            i, n = steps.pop(0)
+            rings[i].step(n)
+
+    turn()
     x0.wait_recv()
     fy = go(4, piece(xn, 0), piece(xn, 0), ydev)
     pass_on(6, xn, 0)
     y1.wait_recv()
     fx = go(5, piece(yn, 1), piece(yn, 1), xdev)
     pass_on(7, yn, 1)
+    own_up = swap(2, up, up_block.at[at(me, rows), :])
+    turn()
+    turn()
     x1.wait_recv()
     pass_on(8, xn, 1)
     y0.wait_recv()
     pass_on(9, yn, 0)
+    turn()
     fy.wait_recv()
     pass_on(10, far, 0)
     fx.wait_recv()
     pass_on(11, far, 1)
-    for c in started:
+    while steps:
+        turn()
+    own_cot.wait()
+    own_up.wait()
+    for c in swaps[2]:
+        c.wait_recv()
+    for c in started + swaps[0] + swaps[1] + swaps[2]:
         c.wait_send()
     for c in passed:
         c.wait()
-
-
-def middle_kernel(g, gate, up, cots, down, hidden, d_gate, d_up, gates, ups, dh, send, recv, own):
+    for r in rings:
+        r.finish()
+
+
+def middle_kernel(g, n_out, gate, up, cots, down, block, hidden, d_gate, d_up, up_all, gates, ups, dh, send, recv, zsend, zrecv, own):
     base, me, core = place(g)
-    greet(peers(g, base, me, core))
+    outer = lax.div(base, g)
+    greet(peers(g, base, me, core) + ring_devices(outer, n_out, me, core, g))
+    first = pltpu.make_async_copy(block, up_all.at[at(outer, block.shape[0]), :], own.at[2])
+    first.start()
     rows, part = gate.shape[0], gate.shape[1] // g
     copies = {}
     for k in range(1, g):
@@ -140,6 +188,9 @@
         c = pltpu.make_async_copy(a.at[:, at(me, part)], b.at[at(me, rows), :], own.at[i])
         c.start()
         copies[i, 0] = c
+    first.wait()
+    ring = Ring(up_all, block.shape[0], outer, n_out, base, me, core, g, zsend, zrecv, 0)
+    ring.step(0)
     tile = rows // 2
 
     def multiply(i, carry):
@@ -147,8 +198,11 @@
         return carry
 
     lax.fori_loop(0, 2 * g, multiply, 0)
+    steps = list(range(1, n_out))
     strip = rows // 16
     for k in range(g):
+        if steps:
+            ring.step(steps.pop(0))
         for i in range(2):
             if k:
                 copies[i, k].wait_recv()
@@ -167,6 +221,9 @@
             return carry
 
         lax.fori_loop(0, 16, pointwise, 0)
+    while steps:
+        ring.step(steps.pop(0))
+    ring.finish()
     for k in range(1, g):
         for i in range(2):
             copies[i, k].wait_send()
@@ -279,27 +336,18 @@
     struct = jax.ShapeDtypeStruct
     us = 3_000_000
     columns = [[o * g + p for o in range(n_out)] for p in range(g)]
-    gather = functools.partial(lax.all_gather, axis_name="fs", axis_index_groups=columns, axis=0, tiled=True)
-
-    def swap(ident, *weights):
-        n = len(weights)
-        return call(
-            functools.partial(swap_kernel, g, n), [struct((rows * g, part), BF16)] * n,
-            [sems((n, g)), sems((n, g)), sems((n,))], ident, 7 * n * us, *weights,
-        )
-
-    down_all = gather(swap(0, down_weight)[0])
-    gate_block, up_block = swap(1, gate_weight, up_weight)
-    up_w = gather(up_block)
-    cots, gate_w = call(
-        functools.partial(tokens_kernel, g, n_out), [struct((all_tokens, depth), BF16), struct((depth, part), BF16)],
-        [sems((12,)), sems((12,)), sems((n_out,)), sems((n_out,)), sems((2,))], 2, 40 * us, cotangent, gate_block,
+    every, block = struct((depth, part), BF16), struct((rows * g, part), BF16)
+    cots, down_all, gate_w, up_block = call(
+        functools.partial(tokens_kernel, g, n_out), [struct((all_tokens, depth), BF16), every, every, block],
+        [sems((12,)), sems((12,)), sems((3, g)), sems((3, g)), sems((2, 2 * n_out)), sems((2, 2 * n_out)), sems((4,))],
+        0, 60 * us, cotangent, down_weight, gate_weight, up_weight,
     )
     wide = struct((all_tokens, part), BF16)
-    hidden, d_gate, d_up = call(
-        functools.partial(middle_kernel, g), [wide] * 3,
-        [vmem(wide.shape, BF16)] * 2 + [vmem(wide.shape, F32), sems((2, g)), sems((2, g)), sems((2,))],
-        3, 40 * us, gate_pre, up_pre, cots, down_all,
+    hidden, d_gate, d_up, up_w = call(
+        functools.partial(middle_kernel, g, n_out), [wide] * 3 + [every],
+        [vmem(wide.shape, BF16)] * 2
+        + [vmem(wide.shape, F32), sems((2, g)), sems((2, g)), sems((1, 2 * n_out)), sems((1, 2 * n_out)), sems((3,))],
+        1, 40 * us, gate_pre, up_pre, cots, down_all, up_block,
     )
     share = lax.dot_general(cots, hidden, (((0,), (0,)), ((), ())), preferred_element_type=F32).astype(BF16)
     grad_block = lax.psum_scatter(share, "fs", scatter_dimension=0, axis_index_groups=columns, tiled=True)
@@ -308,11 +356,11 @@
         functools.partial(input_kernel, g), [struct((tokens, depth), BF16)],
         [vmem((4, tokens, side), BF16)] * 3 + [vmem((2, tokens, side), BF16), vmem((2, tokens // 2, side), BF16)]
         + [sems((12,)), sems((12,))],
-        4, 50 * us, d_gate, d_up, gate_w, up_w,
+        2, 50 * us, d_gate, d_up, gate_w, up_w,
     )[0]
     grad_down = call(
         functools.partial(down_kernel, g), [struct((rows, width), F32)],
-        [vmem((g, rows, part), BF16), sems((g,)), sems((g,))], 5, 6 * us, grad_block,
+        [vmem((g, rows, part), BF16), sems((g,)), sems((g,))], 3, 6 * us, grad_block,
     )[0]
     return grad_input, grad_down
 

time: 215 us -> 201 us (0.935); the launches traced: 215 us -> 199 us
  Pallas kernels: 187 us -> 171 us
    pallas_call x6 -> x4, Pallas kernels: 187 us -> 171 us  [call(): pl.pallas_call(kernel, out_shape=outs, in_specs=[vmem] * len(args), out_s...]
  transfers between devices with their start and end apart: 3 -> 1, of which waited for: 0 -> 0; matrix products, arithmetic and copies ran while one was open for 4% -> 0% of each run, Pallas kernels for 78% -> 24%
where the time goes in v3:
time: 201 us; the launch traced here: 199 us
  Pallas kernels  171 us (85%)
  between operations  14.1 us (7%)
  matrix products  9.51 us (5%)
  local copies, waits for them, and re-layouts  4.12 us (2%)
    pallas_call x4, Pallas kernels, call(): pl.pallas_call(kernel, out_shape=outs, in_specs=[vmem] * len(args), out_s...  171 us
    dot_general x1, matrix products, shared(): lax.dot_general(cots, hidden, (((0,), (0,)), ((), ())), preferred_element...  9.51 us
    unnamed x4, local copies, waits for them, and re-layouts  4.12 us
  transfers between devices with their start and end apart: 1, of which 0 were waited for; matrix products, arithmetic and copies ran while one was open for 0% of the time, Pallas kernels for 24%

profile of v3, /device:TPU:9, one launch (start us, length us, event | category | flops | bytes accessed | tf_op | source)
XLA Modules:
  0.0 198.8 jit_solution(14444898814487626213)
XLA Ops:
  7.2 0.0 reduce-scatter.2.cloned.1.call-start
  7.2 64.2 %shard_map.77 = (bf16[2048,2048]{1,0:T(8,128)(2,1)}, bf16[2048,384]{1,0:T(8,128)(2,1)}, bf16[2048,384]{1,0:T(8,128)(2,1)}, bf16[512,384]{1,0:T(8,128)(2,1)}) custom-call(bf16[512,2048]{1,0:T(8,128)(2,1)} %cot.1, bf16[128,1536]{1,0:T(8,128)(2,1)} %down.1, bf16[128,1536]{1,0:T(8,128)(2,1)} %gate.2, bf16[128,1536]{1,0:T(8,128)(2,1)} %up.2), custom_call_target="tpu_custom_call" | custom-call | bytes 180000000 | tf_op jit(solution)/shard_map/pallas_call | solution.py:320
  71.5 49.7 %shard_map.78 = (bf16[2048,384]{1,0:T(8,128)(2,1)}, bf16[2048,384]{1,0:T(8,128)(2,1)}, bf16[2048,384]{1,0:T(8,128)(2,1)}, bf16[2048,384]{1,0:T(8,128)(2,1)}) custom-call(bf16[512,1536]{1,0:T(8,128)(2,1)} %gate.3, bf16[512,1536]{1,0:T(8,128)(2,1)} %up.3, bf16[2048,2048]{1,0:T(8,128)(2,1)} %get-tuple-element.10.cots, ...), custom_call_target="tpu_custom_call" | custom-call | bytes 120000000 | tf_op jit(solution)/shard_map/pallas_call | solution.py:320
  121.2 9.5 %convolution_convert_fusion = bf16[2048,384]{1,0:T(8,128)(2,1)} fusion(bf16[2048,2048]{1,0:T(8,128)(2,1)} %get-tuple-element.10.cots, bf16[2048,384]{1,0:T(8,128)(2,1)} %get-tuple-element.17), kind=kOutput, calls=%fused_computation | convolution fusion | flops 3222011904 | bytes 11534336 | tf_op jit(solution)/shard_map/dot_general | solution.py:352
  130.7 0.0 reduce-scatter.2.cloned.1.call-update
  130.7 48.0 %shard_map.79 = bf16[512,2048]{1,0:T(8,128)(2,1)} custom-call(bf16[2048,384]{1,0:T(8,128)(2,1)} %get-tuple-element.13.d_gate, bf16[2048,384]{1,0:T(8,128)(2,1)} %get-tuple-element.14.d_up, bf16[2048,384]{1,0:T(8,128)(2,1)} %get-tuple-element.15.gate_w, bf16[2048,384]{1,0:T(8,128)(2,1)} %get-tuple-element.16.up_w), custom_call_target="tpu_custom_call" | custom-call | bytes 150000000 | tf_op jit(solution)/shard_map/pallas_call | solution.py:320
  178.7 0.0 reduce-scatter.2.cloned.1.call-done.down
  178.8 9.0 %shard_map.80 = f32[128,1536]{1,0:T(8,128)} custom-call(bf16[512,384]{1,0:T(8,128)(2,1)} %reduce-scatter.2.cloned.1.call-done.down), custom_call_target="tpu_custom_call" | custom-call | bytes 18000000 | tf_op jit(solution)/shard_map/pallas_call | solution.py:320
  187.8 0.0 copy-start
  187.8 3.2 %copy.10 = bf16[512,2048]{1,0:T(8,128)(2,1)} copy(bf16[512,2048]{1,0:T(8,128)(2,1)} %shard_map.79) | data formatting | bytes 4194304
  191.0 0.0 copy-done
  191.0 0.9 copy.11
Async XLA Ops:
  7.2 171.6 %reduce-scatter.2.cloned.1.call-start = ((), (), s32[]{:S(2)}) async-start(), calls=%async_computation.1 | async-start | bytes 1966080 | tf_op jit(solution)/shard_map/reduce_scatter | solution.py:353
  187.8 3.2 %copy-start = (f32[128,1536]{1,0:T(8,128)S(1)}, f32[128,1536]{1,0:T(8,128)}, u32[]{:S(2)}) copy-start(f32[128,1536]{1,0:T(8,128)} %shard_map.80) | copy-start | bytes 2359300
Sparse Core Ops, SparseCore 0:
  130.9 32.6 reduce-scatter.1

commit v4 on v3

--- a/solution.py
+++ b/solution.py
@@ -170,7 +170,7 @@
         r.finish()
 
 
-def middle_kernel(g, n_out, gate, up, cots, down, block, hidden, d_gate, d_up, up_all, gates, ups, dh, send, recv, zsend, zrecv, own):
+def middle_kernel(g, n_out, gate, up, cots, down, block, share, d_gate, d_up, up_all, gates, ups, dh, hidden, acc, send, recv, zsend, zrecv, own):
     base, me, core = place(g)
     outer = lax.div(base, g)
     greet(peers(g, base, me, core) + ring_devices(outer, n_out, me, core, g))
@@ -221,6 +221,21 @@
             return carry
 
         lax.fori_loop(0, 16, pointwise, 0)
+        tokens = at(owner, rows)
+        piece = cots.shape[1] // 8
+
+        def outer_product(i, carry):
+            d = at(i, piece)
+            new = lax.dot_general(cots[tokens, d], hidden[tokens, :], (((0,), (0,)), ((), ())), preferred_element_type=F32)
+            if k:
+                new = new + acc[d, :]
+            if k == g - 1:
+                share[d, :] = new.astype(BF16)
+            else:
+                acc[d, :] = new
+            return carry
+
+        lax.fori_loop(0, 8, outer_product, 0)
     while steps:
         ring.step(steps.pop(0))
     ring.finish()
@@ -343,13 +358,12 @@
         0, 60 * us, cotangent, down_weight, gate_weight, up_weight,
     )
     wide = struct((all_tokens, part), BF16)
-    hidden, d_gate, d_up, up_w = call(
-        functools.partial(middle_kernel, g, n_out), [wide] * 3 + [every],
+    share, d_gate, d_up, up_w = call(
+        functools.partial(middle_kernel, g, n_out), [every] + [wide] * 2 + [every],
         [vmem(wide.shape, BF16)] * 2
-        + [vmem(wide.shape, F32), sems((2, g)), sems((2, g)), sems((1, 2 * n_out)), sems((1, 2 * n_out)), sems((3,))],
+        + [vmem(wide.shape, F32), vmem(wide.shape, BF16), vmem(every.shape, F32), sems((2, g)), sems((2, g)), sems((1, 2 * n_out)), sems((1, 2 * n_out)), sems((3,))],
         1, 40 * us, gate_pre, up_pre, cots, down_all, up_block,
     )
-    share = lax.dot_general(cots, hidden, (((0,), (0,)), ((), ())), preferred_element_type=F32).astype(BF16)
     grad_block = lax.psum_scatter(share, "fs", scatter_dimension=0, axis_index_groups=columns, tiled=True)
     side = depth // 2
     grad_input = call(

time: 201 us -> 196 us (0.975)
  matrix products: 9.51 us -> 0 us
  Pallas kernels: 171 us -> 176 us
    dot_general x1 -> x0, matrix products: 9.51 us -> none  [shared(): lax.dot_general(cots, hidden, (((0,), (0,)), ((), ())), preferred_element...]
    pallas_call x4, Pallas kernels: 171 us -> 176 us  [call(): pl.pallas_call(kernel, out_shape=outs, in_specs=[vmem] * len(args), out_s...]
  transfers between devices with their start and end apart: 1 -> 1, of which waited for: 0 -> 0; matrix products, arithmetic and copies ran while one was open for 0% -> 0% of each run, Pallas kernels for 24% -> 25%
where the time goes in v4:
time: 196 us; the launch traced here: 194 us
  Pallas kernels  176 us (90%)
  between operations  14.1 us (7%)
  local copies, waits for them, and re-layouts  4.12 us (2%)
    pallas_call x4, Pallas kernels, call(): pl.pallas_call(kernel, out_shape=outs, in_specs=[vmem] * len(args), out_s...  176 us
    unnamed x4, local copies, waits for them, and re-layouts  4.12 us
  transfers between devices with their start and end apart: 1, of which 0 were waited for; matrix products, arithmetic and copies ran while one was open for 0% of the time, Pallas kernels for 25%

profile of v4, /device:TPU:9, one launch (start us, length us, event | category | flops | bytes accessed | tf_op | source)
XLA Modules:
  0.0 194.1 jit_solution(11137093945802676057)
XLA Ops:
  7.2 0.0 reduce-scatter.2.cloned.1.call-start
  7.2 64.2 %shard_map.77 = (bf16[2048,2048]{1,0:T(8,128)(2,1)}, bf16[2048,384]{1,0:T(8,128)(2,1)}, bf16[2048,384]{1,0:T(8,128)(2,1)}, bf16[512,384]{1,0:T(8,128)(2,1)}) custom-call(bf16[512,2048]{1,0:T(8,128)(2,1)} %cot.1, bf16[128,1536]{1,0:T(8,128)(2,1)} %down.1, bf16[128,1536]{1,0:T(8,128)(2,1)} %gate.2, bf16[128,1536]{1,0:T(8,128)(2,1)} %up.2), custom_call_target="tpu_custom_call" | custom-call | bytes 180000000 | tf_op jit(solution)/shard_map/pallas_call | solution.py:335
  71.5 55.0 %shard_map.78 = (bf16[2048,384]{1,0:T(8,128)(2,1)}, bf16[2048,384]{1,0:T(8,128)(2,1)}, bf16[2048,384]{1,0:T(8,128)(2,1)}, bf16[2048,384]{1,0:T(8,128)(2,1)}) custom-call(bf16[512,1536]{1,0:T(8,128)(2,1)} %gate.3, bf16[512,1536]{1,0:T(8,128)(2,1)} %up.3, bf16[2048,2048]{1,0:T(8,128)(2,1)} %get-tuple-element.10.cots, ...), custom_call_target="tpu_custom_call" | custom-call | bytes 120000000 | tf_op jit(solution)/shard_map/pallas_call | solution.py:335
  126.4 0.0 reduce-scatter.2.cloned.1.call-update
  126.5 48.0 %shard_map.79 = bf16[512,2048]{1,0:T(8,128)(2,1)} custom-call(bf16[2048,384]{1,0:T(8,128)(2,1)} %get-tuple-element.13.d_gate, bf16[2048,384]{1,0:T(8,128)(2,1)} %get-tuple-element.14.d_up, bf16[2048,384]{1,0:T(8,128)(2,1)} %get-tuple-element.15.gate_w, bf16[2048,384]{1,0:T(8,128)(2,1)} %get-tuple-element.16.up_w), custom_call_target="tpu_custom_call" | custom-call | bytes 150000000 | tf_op jit(solution)/shard_map/pallas_call | solution.py:335
  174.5 0.0 reduce-scatter.2.cloned.1.call-done.down
  174.5 8.5 %shard_map.80 = f32[128,1536]{1,0:T(8,128)} custom-call(bf16[512,384]{1,0:T(8,128)(2,1)} %reduce-scatter.2.cloned.1.call-done.down), custom_call_target="tpu_custom_call" | custom-call | bytes 18000000 | tf_op jit(solution)/shard_map/pallas_call | solution.py:335
  183.1 0.0 copy-start
  183.1 3.2 %copy.10 = bf16[512,2048]{1,0:T(8,128)(2,1)} copy(bf16[512,2048]{1,0:T(8,128)(2,1)} %shard_map.79) | data formatting | bytes 4194304
  186.3 0.0 copy-done
  186.3 0.9 copy.11
Async XLA Ops:
  7.2 167.4 %reduce-scatter.2.cloned.1.call-start = ((), (), s32[]{:S(2)}) async-start(), calls=%async_computation.1 | async-start | bytes 1966080 | tf_op jit(solution)/shard_map/reduce_scatter | solution.py:367
  183.1 3.2 %copy-start = (f32[128,1536]{1,0:T(8,128)S(1)}, f32[128,1536]{1,0:T(8,128)}, u32[]{:S(2)}) copy-start(f32[128,1536]{1,0:T(8,128)} %shard_map.80) | copy-start | bytes 2359300
Sparse Core Ops, SparseCore 0:
  126.6 32.3 reduce-scatter.1
